TPU v7x, 32 devices: a whole 2x2x4 slice. The times are simulated.
32 devices in a mesh: grp: 2 (over y), fs: 4 (over z), tp: 4 (over x, core).
Axes of the slice: x: 2, y: 2, z: 4, core: 2. Of those that a mesh axis runs over, the one named last changes fastest.
Arguments:
- tokens: bfloat16 [6144, 2048], P(('grp', 'fs'), 'tp'), parts along dimension 0, may hold values from -6 to 6
- recurrent_norm_gain: float32 [2048], replicated, may hold values from 0.1 to 1.9
- channel_norm_gain: float32 [2048], replicated, may hold values from 0.1 to 1.9
- gate_projection_weight: float32 [2048, 2048], P('fs', 'tp'), may hold values from -0.125 to 0.125
- gate_column_scale: float32 [2048], P(('tp', 'fs')), may hold values from 0.5 to 2
- input_projection_weight: float32 [2048, 2048], P('fs', 'tp'), may hold values from -0.125 to 0.125
- input_column_scale: float32 [2048], P(('tp', 'fs')), may hold values from 0.5 to 2
- convolution_kernel: float32 [4, 2048], P(None, 'tp'), may hold values from -3 to 3
- recurrence_gate_weight: float32 [8, 256, 256], P('tp', 'fs'), may hold values from -0.375 to 0.375
- recurrence_column_scale: float32 [8, 256], P('tp', 'fs'), may hold values from 0.25 to 4
- input_gate_weight: float32 [8, 256, 256], P('tp', 'fs'), may hold values from -0.375 to 0.375
- input_gate_column_scale: float32 [8, 256], P('tp', 'fs'), may hold values from 0.5 to 2
- channel_decay_param: float32 [2048], P('tp'), may hold values from 2.2 to 8.5
- position_decay_shift: float32 [6144], P(('grp', 'fs')), parts along dimension 0, may hold values from -0.7 to 0
- output_projection_weight: float32 [2048, 2048], P('tp', 'fs'), may hold values from -0.125 to 0.125
- output_column_scale: float32 [2048], P('fs'), may hold values from 0.5 to 2
- mixer_gate_weight: float32 [2048, 5632], P('fs', 'tp'), may hold values from -0.125 to 0.125
- mixer_gate_column_scale: float32 [5632], P(('tp', 'fs')), may hold values from 0.5 to 2
- up_projection_weight: float32 [2048, 5632], P('fs', 'tp'), may hold values from -0.125 to 0.125
- up_column_scale: float32 [5632], P(('tp', 'fs')), may hold values from 0.5 to 2
- down_projection_weight: float32 [5632, 2048], P('tp', 'fs'), may hold values from -0.078125 to 0.078125
- down_column_scale: float32 [2048], P('fs'), may hold values from 0.5 to 2
Outputs:
- layer_out: bfloat16 [6144, 2048], P(('grp', 'fs'), 'tp'), parts along dimension 0
There are 2 independent parts, one for each index of `grp`. A program takes and returns all parts, laid end to end along the dimension named above; an argument that names none is the same for every part. Nothing has to cross between parts.
All inputs are finite; a program needn't handle non-finite values.
Results may differ from a plain program's by a relative error of at most 0.023.
Values may be sent and summed in bfloat16 or wider, within the bound.
A program may use at most 128 MiB of HBM per device.

v0:
```python
import jax
import jax.numpy as jnp
from jax import lax
from jax.experimental import pallas as pl
from jax.experimental.pallas import tpu as pltpu
from jax.sharding import PartitionSpec as P

TAPS = 4
SEQ_LEN = 128
LANES = 128
MESH = pl.DeviceIdType.MESH

eps = 1e-06


def shares(total, parts):
    parts = min(parts, total)
    return [total // parts + (1 if i < total % parts else 0) for i in range(parts)]


def ring_plan(costs, count, latency):
    ready = {(c, 0): 0.0 for c in range(len(costs))}
    free, plan, landed = 0.0, [], {}
    while ready:
        at_hand = [k for k in ready if ready[k] <= free]
        if not at_hand:
            free = min(ready.values())
            continue
        c, s = min(at_hand, key=lambda k: (k[0], -k[1]))
        begin = free
        del ready[(c, s)]
        free = free + costs[c]
        landed[(c, s)] = free + latency
        plan.append((begin, c, s))
        if s + 1 < count - 1:
            ready[(c, s + 1)] = free + latency
    for c in range(len(costs)):
        plan.append((landed[(c, count - 2)], c, count - 1))
    return sorted(plan), landed


def layer_body(dims, *refs):
    (n, copies, tp, rows, model, dc, rec, blocks, brows, width, hid, col) = dims
    (
        tokens, wpair, wblk, wout, wff, wdn, scales, gain1, gain2, taps, decay, shift, out,
        Wp, Wb, Wo, Wf, Wd, X, H, N, UG, M, T1, R1, T2, R2, A, S, SV,
        z_send, z_recv, y_send, y_recv, own_sem, tok_sem,
        x_send, x_recv, r1_send, r1_recv, h_send, h_recv, r2_send, r2_recv, s_send, s_recv,
    ) = refs
    g, f, t = lax.axis_index("grp"), lax.axis_index("fs"), lax.axis_index("tp")
    krows = model // n

    barrier = pltpu.get_barrier_semaphore()
    for axis, count, here in (("fs", n, f), ("grp", copies, g), ("tp", tp, t)):
        for k in range(1, count):
            pl.semaphore_signal(
                barrier, inc=1, device_id={axis: lax.rem(here + k, count)}, device_id_type=MESH
            )

    def remote(src, dst, send, recv, axis, index):
        return pltpu.make_async_remote_copy(
            src_ref=src, dst_ref=dst, send_sem=send, recv_sem=recv,
            device_id={axis: index}, device_id_type=MESH,
        )

    chunks, tags = [], {}

    def by_rows(buf, source, first, wide):
        per = krows // copies

        def view(owner, share):
            return buf.at[pl.ds(pl.multiple_of(owner * krows + share * per, per), per), pl.ds(first, wide)]

        return (
            view,
            source.at[:, pl.ds(first, wide)],
            lambda: buf.at[pl.ds(pl.multiple_of(f * krows, krows), krows), pl.ds(first, wide)],
            per * wide,
        )

    def by_columns(buf, source, first, wide):
        deep = buf.shape[0]
        per = deep // copies

        def view(owner, share):
            return buf.at[
                pl.ds(pl.multiple_of(share * per, per), per),
                pl.ds(pl.multiple_of(owner * col + first, LANES), wide),
            ]

        return (
            view,
            source.at[:, pl.ds(first, wide)],
            lambda: buf.at[:, pl.ds(pl.multiple_of(f * col + first, LANES), wide)],
            per * wide,
        )

    def by_blocks():
        per = 2 * width // copies

        def view(owner, share):
            return Wb.at[
                :, pl.ds(pl.multiple_of(owner * brows, brows), brows),
                pl.ds(pl.multiple_of(share * per, per), per),
            ]

        return (
            view,
            wblk,
            lambda: Wb.at[:, pl.ds(pl.multiple_of(f * brows, brows), brows), :],
            blocks * brows * per,
        )

    def add(tag, chunk):
        tags[tag] = len(chunks)
        chunks.append(chunk)

    add("in", by_rows(Wp, wpair, rec, rec))
    add("blk", by_blocks())
    add("gate", by_rows(Wp, wpair, 0, rec))
    add("out", by_columns(Wo, wout, 0, col))
    ff_groups, first = [], 0
    for pairs in shares(hid // LANES, 4):
        add(("ff", len(ff_groups)), by_rows(Wf, wff, first * 2 * LANES, pairs * 2 * LANES))
        ff_groups.append((first, pairs))
        first += pairs
    dn_groups, first = [], 0
    for lanes in shares(col // LANES, 3):
        add(("dn", len(dn_groups)), by_columns(Wd, wdn, first * LANES, lanes * LANES))
        dn_groups.append((first * LANES, lanes * LANES))
        first += lanes

    own = []
    for c, (view, source, place, cost) in enumerate(chunks):
        own.append(pltpu.make_async_copy(source, place(), own_sem.at[c]))
        own[c].start()
    tok = pltpu.make_async_copy(tokens, X.at[t], tok_sem.at[0])
    tok.start()
    S[f] = scales[...]

    pl.semaphore_wait(barrier, (n - 1) + (copies - 1) + (tp - 1))

    drains = []

    def send(copy):
        copy.start()
        drains.append(copy)

    def z_copy(c, s):
        owner = lax.rem(f - s + n, n)
        view = chunks[c][0](owner, g)
        return remote(view, view, z_send.at[c, s], z_recv.at[c, s], "fs", lax.rem(f + 1, n))

    def z_land(c, s):
        owner = lax.rem(f - s - 1 + n, n)
        view = chunks[c][0](owner, g)
        return remote(view, view, z_send.at[c, s], z_recv.at[c, s], "fs", lax.rem(f + 1, n))

    def y_copy(c, s, other, share):
        owner = lax.rem(f - s + n, n)
        view = chunks[c][0](owner, share)
        return remote(
            view, view, y_send.at[c, s - 1, other - 1], y_recv.at[c, s - 1, other - 1],
            "grp", lax.rem(g + other, copies),
        )

    def ring_step(c, s):
        if s == 0:
            own[c].wait()
        else:
            z_land(c, s - 1).wait_recv()
        if s < n - 1:
            send(z_copy(c, s))
        if s > 0:
            for other in range(1, copies):
                send(y_copy(c, s, other, g))

    def settled(c, s):
        for other in range(1, copies):
            y_copy(c, s, other, lax.rem(g - other + copies, copies)).wait_recv()

    def gathered(c):
        for s in range(1, n):
            settled(c, s)

    def spread(source, buf, sends, recvs):
        for k in range(1, tp):
            send(remote(source, buf.at[t], sends.at[k - 1], recvs.at[k - 1], "tp", lax.rem(t + k, tp)))

    def spread_land(buf, sends, recvs):
        for k in range(1, tp):
            place = buf.at[lax.rem(t - k + tp, tp)]
            remote(place, place, sends.at[k - 1], recvs.at[k - 1], "tp", lax.rem(t + k, tp)).wait_recv()

    spread(tokens, X, x_send, x_recv)
    for k in range(1, n):
        send(remote(scales, S.at[f], s_send.at[k - 1], s_recv.at[k - 1], "fs", lax.rem(f + k, n)))

    def norm(buf, gain):
        def tile(i, _):
            here = pl.ds(pl.multiple_of(i * SEQ_LEN, SEQ_LEN), SEQ_LEN)
            parts = [buf[p, here, :].astype(jnp.float32) for p in range(tp)]
            total = sum(jnp.sum(v * v, axis=-1, keepdims=True) for v in parts)
            factor = lax.rsqrt(total / model + eps)
            for p in range(tp):
                lanes = slice(p * dc, (p + 1) * dc)
                N[here, lanes] = (parts[p] * factor * gain[:, lanes]).astype(jnp.bfloat16)
            return 0

        lax.fori_loop(0, rows // SEQ_LEN, tile, 0)

    def first_norm():
        tok.wait()
        spread_land(X, x_send, x_recv)
        norm(X, gain1)

    def project(tag, first):
        def run():
            gathered(tags[tag])

            def tile(i, _):
                lanes = pl.ds(pl.multiple_of(first + i * 256, LANES), 256)
                summed = jnp.dot(N[...], Wp[:, lanes], preferred_element_type=jnp.float32)
                UG[:, lanes] = (summed * SV[:, lanes]).astype(jnp.bfloat16)
                return 0

            lax.fori_loop(0, rec // 256, tile, 0)

        return run

    def scale_sum():
        for k in range(1, n):
            place = S.at[lax.rem(f - k + n, n)]
            remote(place, place, s_send.at[k - 1], s_recv.at[k - 1], "fs", lax.rem(f + k, n)).wait_recv()
        total = S[0]
        for o in range(1, n):
            total = total + S[o]
        SV[...] = total

    def recurrence():
        gathered(tags["blk"])
        position = lax.broadcasted_iota(jnp.int32, (SEQ_LEN, width), 0)

        def sequence(i, _):
            here = pl.ds(pl.multiple_of(i * SEQ_LEN, SEQ_LEN), SEQ_LEN)
            moved_by = shift[here, :]
            for block in range(blocks):
                lanes = slice(block * width, (block + 1) * width)
                at = lambda base: slice(base + block * width, base + (block + 1) * width)
                branch = UG[here, at(rec)].astype(jnp.float32)
                summed = branch * taps[0:1, lanes]
                for offset in range(1, TAPS):
                    moved = jnp.where(position >= offset, pltpu.roll(branch, offset, 0), 0.0)
                    summed = summed + moved * taps[offset : offset + 1, lanes]
                conv = summed.astype(jnp.bfloat16)
                sums = jnp.dot(conv, Wb[block], preferred_element_type=jnp.float32)
                recur = jax.nn.sigmoid(sums[:, :width] * SV[:, at(2 * rec)])
                inject = jax.nn.sigmoid(sums[:, width:] * SV[:, at(3 * rec)])
                log_keep = -8.0 * recur * decay[:, lanes] + moved_by
                twice = 2.0 * log_keep
                near = -twice * (
                    1.0
                    + twice * (0.5 + twice * (1.0 / 6 + twice * (1.0 / 24 + twice * (1.0 / 120))))
                )
                lost = jnp.where(twice > -0.125, near, 1.0 - jnp.exp(twice))
                factor = jnp.where(position == 0, 1.0, jnp.sqrt(lost))
                state = conv.astype(jnp.float32) * inject * factor
                keep = jnp.exp(log_keep)
                reach = 1
                while reach < SEQ_LEN:
                    inside = position >= reach
                    state = state + keep * jnp.where(inside, pltpu.roll(state, reach, 0), 0.0)
                    keep = keep * jnp.where(inside, pltpu.roll(keep, reach, 0), 1.0)
                    reach *= 2
                gate = UG[here, lanes].astype(jnp.float32)
                M[here, lanes] = (jax.nn.gelu(gate) * state).astype(jnp.bfloat16)
            return 0

        lax.fori_loop(0, rows // SEQ_LEN, sequence, 0)

    def mix_out():
        gathered(tags["out"])
        for k in list(range(1, tp)) + [0]:
            peer = lax.rem(t + k, tp)
            lanes = pl.ds(pl.multiple_of(peer * dc, dc), dc)
            T1[k] = jnp.dot(M[...], Wo[:, lanes], preferred_element_type=jnp.float32).astype(jnp.bfloat16)
            if k:
                send(remote(T1.at[k], R1.at[k - 1], r1_send.at[k - 1], r1_recv.at[k - 1], "tp", peer))

    def hidden():
        for k in range(1, tp):
            place = R1.at[k - 1]
            remote(place, place, r1_send.at[k - 1], r1_recv.at[k - 1], "tp", lax.rem(t + k, tp)).wait_recv()

        def tile(i, _):
            here = pl.ds(pl.multiple_of(i * SEQ_LEN, SEQ_LEN), SEQ_LEN)
            total = T1[0, here, :].astype(jnp.float32)
            for k in range(1, tp):
                total = total + R1[k - 1, here, :].astype(jnp.float32)
            H[t, here, :] = (X[t, here, :].astype(jnp.float32) + total).astype(jnp.bfloat16)
            return 0

        lax.fori_loop(0, rows // SEQ_LEN, tile, 0)
        spread(H.at[t], H, h_send, h_recv)

    def second_norm():
        spread_land(H, h_send, h_recv)
        norm(H, gain2)

    def activate(index):
        first, pairs = ff_groups[index]

        def run():
            gathered(tags[("ff", index)])

            def tile(i, _):
                both = pl.ds(pl.multiple_of((first + i) * 2 * LANES, 2 * LANES), 2 * LANES)
                cols = pl.ds(pl.multiple_of(4 * rec + (first + i) * 2 * LANES, LANES), 2 * LANES)
                summed = jnp.dot(N[...], Wf[:, both], preferred_element_type=jnp.float32)
                summed = summed * SV[:, cols]
                one = pl.ds(pl.multiple_of((first + i) * LANES, LANES), LANES)
                A[:, one] = (jax.nn.silu(summed[:, :LANES]) * summed[:, LANES:]).astype(jnp.bfloat16)
                return 0

            lax.fori_loop(0, pairs, tile, 0)

        return run

    pieces = []

    def down(index, s):
        first, wide = dn_groups[index]

        def run():
            if s:
                settled(tags[("dn", index)], s)
            start = lax.rem(f - s + n, n) * col + first
            lanes = pl.ds(pl.multiple_of(start, LANES), wide)
            peer = start // dc
            inner = start - peer * dc
            T2[:, lanes] = jnp.dot(A[...], Wd[:, lanes], preferred_element_type=jnp.float32).astype(jnp.bfloat16)

            def piece():
                return remote(
                    T2.at[:, lanes], R2.at[t, :, pl.ds(pl.multiple_of(inner, LANES), wide)],
                    r2_send.at[index, s], r2_recv.at[t, inner // LANES], "tp", peer,
                )

            @pl.when(peer != t)
            def _():
                piece().start()

            pieces.append((peer, piece))

        return run

    def finish():
        for k in range(1, tp):
            peer = lax.rem(t + k, tp)
            for part in range(dc // col):
                for first, wide in dn_groups:
                    inner = part * col + first
                    place = R2.at[peer, :, pl.ds(inner, wide)]
                    remote(place, place, r2_send.at[0, 0], r2_recv.at[peer, inner // LANES], "tp", peer).wait_recv()

        def tile(i, _):
            here = pl.ds(pl.multiple_of(i * SEQ_LEN, SEQ_LEN), SEQ_LEN)
            total = T2[here, pl.ds(pl.multiple_of(t * dc, dc), dc)].astype(jnp.float32)
            for k in range(1, tp):
                total = total + R2[lax.rem(t + k, tp), here, :].astype(jnp.float32)
            out[here, :] = (H[t, here, :].astype(jnp.float32) + total).astype(jnp.bfloat16)
            return 0

        lax.fori_loop(0, rows // SEQ_LEN, tile, 0)

    link = 2 * 2 / 91e3
    costs = [chunk[3] * link for chunk in chunks]
    ring, landed = ring_plan(costs, n, 6.0)
    events = [(when, 0, c, s, None) for when, c, s in ring]

    def ready(tag, s=None):
        c = tags[tag]
        return landed[(c, (n if s is None else s + 1) - 2)] + costs[c] + 3.0

    clock = [0.0]

    def task(when, takes, run):
        clock[0] = max(clock[0], when)
        events.append((clock[0], 1, len(events), 0, run))
        clock[0] += takes

    across = tp * rows * dc * link / 1.0
    task(1.0, 0.5, scale_sum)
    task(across, 3.0, first_norm)
    task(ready("in"), 3.5, project("in", rec))
    task(ready("gate"), 3.5, project("gate", 0))
    task(ready("blk"), 7.0, recurrence)
    task(ready("out"), 4.0, mix_out)
    task(clock[0] + across, 2.0, hidden)
    task(clock[0] + across, 3.0, second_norm)
    for index in range(len(ff_groups)):
        task(ready(("ff", index)), 7.0, activate(index))
    for index in range(len(dn_groups)):
        for s in range(n):
            task(ready(("dn", index), s) if s else 0.0, 1.5, down(index, s))
    for _, kind, c, s, run in sorted(events, key=lambda e: e[:4]):
        if kind == 0:
            ring_step(c, s)
        else:
            run()
    finish()
    for copy in drains:
        copy.wait_send()
    for peer, piece in pieces:
        @pl.when(peer != t)
        def _(piece=piece):
            piece().wait_send()


def on_device(
    tokens,
    recurrent_norm_gain,
    channel_norm_gain,
    gate_projection_weight,
    gate_column_scale,
    input_projection_weight,
    input_column_scale,
    convolution_kernel,
    recurrence_gate_weight,
    recurrence_column_scale,
    input_gate_weight,
    input_gate_column_scale,
    channel_decay_param,
    position_decay_shift,
    output_projection_weight,
    output_column_scale,
    mixer_gate_weight,
    mixer_gate_column_scale,
    up_projection_weight,
    up_column_scale,
    down_projection_weight,
    down_column_scale,
):
    n, copies, tp = (lax.axis_size(axis) for axis in ("fs", "grp", "tp"))
    f = lax.axis_index("fs")
    narrow = lambda weight: weight.astype(jnp.bfloat16)
    rows, dc = tokens.shape
    model = dc * tp
    krows, rec = gate_projection_weight.shape
    blocks, brows, width = recurrence_gate_weight.shape
    ff = mixer_gate_weight.shape[1]
    hid = -(-ff // LANES) * LANES
    col = output_projection_weight.shape[1]

    def wide(scale):
        kept = scale.reshape(-1, 1, scale.shape[-1])
        owner = lax.broadcasted_iota(jnp.int32, (1, n, 1), 1)
        return jnp.where(owner == f, kept, 0.0).reshape(1, -1)

    def pairs(a, b):
        pad = ((0, 0), (0, hid - ff))
        a, b = (jnp.pad(v, pad).reshape(v.shape[0], -1, 1, LANES) for v in (a, b))
        return jnp.concatenate([a, b], axis=2).reshape(a.shape[0], -1)

    scales = jnp.concatenate(
        [
            wide(gate_column_scale),
            wide(input_column_scale),
            wide(recurrence_column_scale),
            wide(input_gate_column_scale),
            pairs(wide(mixer_gate_column_scale), wide(up_column_scale)),
        ],
        axis=1,
    )
    wpair = jnp.concatenate([narrow(gate_projection_weight), narrow(input_projection_weight)], axis=1)
    wblk = jnp.concatenate([narrow(recurrence_gate_weight), narrow(input_gate_weight)], axis=2)
    wout = narrow(output_projection_weight * output_column_scale)
    wff = pairs(narrow(mixer_gate_weight), narrow(up_projection_weight))
    wdn = jnp.pad(narrow(down_projection_weight * down_column_scale), ((0, hid - ff), (0, 0)))

    dims = (n, copies, tp, rows, model, dc, rec, blocks, brows, width, hid, col)
    chunk_count = 4 + len(shares(hid // LANES, 4)) + len(shares(col // LANES, 3))
    here = pl.BlockSpec(memory_space=pltpu.VMEM)
    away = pl.BlockSpec(memory_space=pl.ANY)
    bf = lambda *shape: pltpu.VMEM(shape, jnp.bfloat16)
    dma = lambda *shape: pltpu.SemaphoreType.DMA(shape)
    flops = 2 * rows * (model * (2 * rec + 2 * hid) + rec * 2 * width + rec * model + hid * model)
    return pl.pallas_call(
        lambda *refs: layer_body(dims, *refs),
        out_shape=jax.ShapeDtypeStruct((rows, dc), jnp.bfloat16),
        in_specs=[away] * 6 + [here] * 6,
        out_specs=here,
        scratch_shapes=[
            bf(model, 2 * rec),
            bf(blocks, n * brows, 2 * width),
            bf(rec, model),
            bf(model, 2 * hid),
            bf(hid, model),
            bf(tp, rows, dc),
            bf(tp, rows, dc),
            bf(rows, model),
            bf(rows, 2 * rec),
            bf(rows, rec),
            bf(tp, rows, dc),
            bf(tp - 1, rows, dc),
            bf(rows, model),
            bf(tp, rows, dc),
            bf(rows, hid),
            pltpu.VMEM((n,) + scales.shape, jnp.float32),
            pltpu.VMEM(scales.shape, jnp.float32),
            dma(chunk_count, n - 1),
            dma(chunk_count, n - 1),
            dma(chunk_count, n - 1, copies - 1),
            dma(chunk_count, n - 1, copies - 1),
            dma(chunk_count),
            dma(1),
            dma(tp - 1),
            dma(tp - 1),
            dma(tp - 1),
            dma(tp - 1),
            dma(tp - 1),
            dma(tp - 1),
            dma(len(shares(col // LANES, 3)), n),
            dma(tp, dc // LANES),
            dma(n - 1),
            dma(n - 1),
        ],
        compiler_params=pltpu.CompilerParams(
            collective_id=0, has_side_effects=True, vmem_limit_bytes=67_043_328
        ),
        cost_estimate=pl.CostEstimate(flops=flops, bytes_accessed=8 * rows * model, transcendentals=0),
    )(
        tokens,
        wpair,
        wblk,
        wout,
        wff,
        wdn,
        scales,
        recurrent_norm_gain[None, :],
        channel_norm_gain[None, :],
        convolution_kernel,
        jax.nn.softplus(-channel_decay_param)[None, :],
        position_decay_shift[:, None],
    )


def solution(mesh):
    placed = (
        P(("grp", "fs"), "tp"),
        P(),
        P(),
        P("fs", "tp"),
        P(("tp", "fs")),
        P("fs", "tp"),
        P(("tp", "fs")),
        P(None, "tp"),
        P("tp", "fs", None),
        P("tp", "fs"),
        P("tp", "fs", None),
        P("tp", "fs"),
        P("tp"),
        P(("grp", "fs")),
        P("tp", "fs"),
        P("fs"),
        P("fs", "tp"),
        P(("tp", "fs")),
        P("fs", "tp"),
        P(("tp", "fs")),
        P("tp", "fs"),
        P("fs"),
    )
    return jax.shard_map(
        on_device, mesh=mesh, in_specs=placed, out_specs=P(("grp", "fs"), "tp"), check_vma=False
    )
```

profile of v0, /device:TPU:5, one launch (start us, length us, event | category | flops | bytes accessed | tf_op | source)
XLA Modules:
  0.0 292.8 jit_solution(10409775376796610945)
XLA Ops:
  0.0 0.0 copy-start
  0.0 0.1 broadcast_bitcast_fusion
  0.1 0.8 broadcast_in_dim.115
  0.9 0.7 broadcast_in_dim.118
  1.6 0.8 broadcast_select_fusion.2
  2.3 0.1 select_n.84
  2.4 0.1 select_n.86
  2.5 0.1 broadcast_in_dim.124
  2.6 0.1 broadcast_in_dim.125
  2.7 0.7 broadcast_in_dim.126
  3.4 0.1 broadcast_in_dim.127
  3.5 0.7 broadcast_in_dim.129
  4.1 0.1 broadcast_in_dim.130
  4.3 0.0 copy-start.11
  4.3 3.0 %copy.30 = bf16[512,1408]{0,1:T(8,128)(2,1)} copy(f32[512,1408]{1,0:T(8,128)} %param.38) | data formatting | bytes 4325376 | tf_op args[16]
  7.3 0.0 copy-done
  7.3 1.6 copy.31
  8.9 0.0 copy-done.11
  8.9 2.1 pad_maximum_fusion
  11.0 5.5 %copy.32 = bf16[512,11,2,128]{3,2,1,0:T(2,128)(2,1)} copy(bf16[512,11,2,128]{0,3,1,2:T(8,128)(2,1)S(1)} %pad_maximum_fusion) | data formatting | bytes 5767168 | tf_op jit(solution)/shard_map/concatenate | solution.py:463
  16.5 0.0 copy-start.2
  16.5 0.0 copy-start.3
  16.5 7.6 %reshape.213.refs_4_ = bf16[512,2816]{1,0:T(8,128)(2,1)} reshape(bf16[512,11,2,128]{3,2,1,0:T(2,128)(2,1)} %copy.32) | data formatting | bytes 5767168 | tf_op jit(solution)/shard_map/reshape | solution.py:463
  24.1 0.0 copy-done.2
  24.1 0.0 copy-start.1
  24.1 0.0 copy-start.8
  24.1 0.1 convert_element_type.24
  24.2 0.0 copy-done.3
  24.2 0.1 convert_element_type.25
  24.2 0.0 copy-start.4
  24.3 0.0 copy-start.9
  24.3 1.1 pad_maximum_fusion.1.refs_1_
  25.4 0.9 copy-done.1
  26.3 0.0 copy-done.8
  26.3 0.0 copy-start.7
  26.3 0.0 copy-start.5
  26.3 0.0 copy-start.6
  26.3 0.0 copy-start.10
  26.3 1.5 multiply_convert_fusion.refs_5_
  27.8 0.0 copy-done.4
  27.8 0.0 copy-done.9
  27.8 0.9 multiply_convert_fusion.1.refs_3_
  28.7 0.0 copy-done.7
  28.7 0.9 broadcast_in_dim.135.refs_11_
  29.7 0.0 copy-done.5
  29.7 0.0 copy-done.6
  29.7 0.7 pad_maximum_fusion.2.refs_2_
  30.4 0.0 copy-done.10
  30.4 0.6 compare_select_fusion
  31.0 259.7 %shard_map.208 = bf16[768,512]{1,0:T(8,128)(2,1)} custom-call(bf16[768,512]{1,0:T(8,128)(2,1)} %refs_0_.1, bf16[512,1024]{1,0:T(8,128)(2,1)} %pad_maximum_fusion.1.refs_1_, bf16[2,64,512]{2,1,0:T(8,128)(2,1)} %pad_maximum_fusion.2.refs_2_, bf16[512,512]{1,0:T(8,128)(2,1)} %multiply_convert_fusion.1.refs_3_, bf16[512,2816]{1,0:T(8,128)(2,1)} %reshape.213.refs_4_, ...), custom_call_target="tpu_custom_call" | custom-call | flops 18522046464 | bytes 12582912 | tf_op jit(solution)/shard_map/pallas_call | solution.py:488
  290.7 2.1 copy.47
  (11 shorter events, 0.1 us)
Async XLA Ops:
  0.0 7.3 %copy-start = (f32[512,1408]{1,0:T(8,128)S(1)}, f32[512,1408]{1,0:T(8,128)}, u32[]{:S(2)}) copy-start(f32[512,1408]{1,0:T(8,128)} %param.40) | copy-start | bytes 8650756
  4.3 4.6 %copy-start.11 = (f32[1,4864]{1,0:T(1,128)}, f32[1,4864]{1,0:T(1,128)S(1)}, u32[]{:S(2)}) copy-start(f32[1,4864]{1,0:T(1,128)S(1)} %constant_dynamic-update-slice_fusion.refs_6_) | copy-start | bytes 58372
  16.5 7.6 %copy-start.2 = (f32[512,512]{1,0:T(8,128)S(1)}, f32[512,512]{1,0:T(8,128)}, u32[]{:S(2)}) copy-start(f32[512,512]{1,0:T(8,128)} %param.25) | copy-start | bytes 3145732
  16.5 7.6 %copy-start.3 = (f32[512,512]{1,0:T(8,128)S(1)}, f32[512,512]{1,0:T(8,128)}, u32[]{:S(2)}) copy-start(f32[512,512]{1,0:T(8,128)} %param.27) | copy-start | bytes 3145732
  24.1 2.2 copy-start.1
  24.1 2.2 copy-start.8
  24.2 3.6 %copy-start.4 = (f32[512,512]{1,0:T(8,128)S(1)}, f32[512,512]{1,0:T(8,128)}, u32[]{:S(2)}) copy-start(f32[512,512]{1,0:T(8,128)} %param.36) | copy-start | bytes 3145732
  24.3 3.6 %copy-start.9 = (f32[512]{0:T(512)S(1)}, f32[512]{0:T(512)}, u32[]{:S(2)}) copy-start(f32[512]{0:T(512)} %param.37) | copy-start | bytes 6148
  26.3 2.5 copy-start.7
  26.3 3.4 %copy-start.5 = (f32[2,64,256]{2,1,0:T(8,128)S(1)}, f32[2,64,256]{2,1,0:T(8,128)}, u32[]{:S(2)}) copy-start(f32[2,64,256]{2,1,0:T(8,128)} %param.30) | copy-start | bytes 393220
  26.3 3.4 %copy-start.6 = (f32[2,64,256]{2,1,0:T(8,128)S(1)}, f32[2,64,256]{2,1,0:T(8,128)}, u32[]{:S(2)}) copy-start(f32[2,64,256]{2,1,0:T(8,128)} %param.32) | copy-start | bytes 393220
  26.3 4.1 %copy-start.10 = (f32[512]{0:T(512)S(1)}, f32[512]{0:T(512)}, u32[]{:S(2)}) copy-start(f32[512]{0:T(512)} %param.34) | copy-start | bytes 6148
where the time goes:
time: 293 us
  Pallas kernels  260 us (89%)
  local copies, waits for them, and re-layouts  25.1 us (9%)
  other arithmetic  7.84 us (3%)
    pallas_call x1, Pallas kernels, on_device(): pl.pallas_call(lambda *refs: layer_body(dims, *refs), out_shape=jax.Shape...  260 us
    unnamed x30, local copies, waits for them, and re-layouts  7.72 us
    reshape x1, local copies, waits for them, and re-layouts, pairs(): return jnp.concatenate([a, b], axis=2).reshape(a.shape[0], -1)  7.56 us

commit v1 on v0

--- a/solution.py
+++ b/solution.py
@@ -8,6 +8,7 @@
 TAPS = 4
 SEQ_LEN = 128
 LANES = 128
+TILE = 64
 MESH = pl.DeviceIdType.MESH
 
 eps = 1e-06
@@ -36,17 +37,23 @@
             ready[(c, s + 1)] = free + latency
     for c in range(len(costs)):
         plan.append((landed[(c, count - 2)], c, count - 1))
-    return sorted(plan), landed
+    passed, free = {}, 0.0
+    for when, c, s in sorted((landed[k], k[0], k[1] + 1) for k in landed):
+        free = max(free, when) + costs[c]
+        passed[(c, s)] = free + latency
+    return sorted(plan), passed
 
 
 def layer_body(dims, *refs):
-    (n, copies, tp, rows, model, dc, rec, blocks, brows, width, hid, col) = dims
-    (
-        tokens, wpair, wblk, wout, wff, wdn, scales, gain1, gain2, taps, decay, shift, out,
-        Wp, Wb, Wo, Wf, Wd, X, H, N, UG, M, T1, R1, T2, R2, A, S, SV,
+    (n, copies, tp, rows, model, dc, rec, blocks, brows, width, ff, hid, col) = dims
+    tokens, weights, (
+        out_scale, down_scale, gate_scale, in_scale, recur_scale, inject_scale, swish_scale, up_scale,
+        gain1, gain2, taps, decay_param, shift, out,
+        Fg, Fi, Fr, Fj, Fo, Fs, Fu, Fd,
+        Wp, Wb, Wo, Wf, Wd, X, H, N, UG, M, T, R1, R2, A, S, SV, SP, Z,
         z_send, z_recv, y_send, y_recv, own_sem, tok_sem,
         x_send, x_recv, r1_send, r1_recv, h_send, h_recv, r2_send, r2_recv, s_send, s_recv,
-    ) = refs
+    ) = refs[0], refs[1:9], refs[9:]
     g, f, t = lax.axis_index("grp"), lax.axis_index("fs"), lax.axis_index("tp")
     krows = model // n
 
@@ -63,23 +70,49 @@
             device_id={axis: index}, device_id_type=MESH,
         )
 
+    staged = (Fi, Fr, Fj, Fg, Fo, Fs, Fu, Fd)
+    loads = {}
+    for k, (source, place) in sorted(enumerate(zip(weights, staged)), key=lambda e: (e[0] not in (1, 2), e[0])):
+        loads[k] = pltpu.make_async_copy(source, place, own_sem.at[k])
+        loads[k].start()
+    tok = pltpu.make_async_copy(tokens, X.at[t], tok_sem.at[0])
+    tok.start()
+
+    def loaded(*which):
+        for k in which:
+            if k in loads:
+                loads.pop(k).wait()
+
+    def by_tiles(total, step, run):
+        def tile(i, _):
+            run(pl.multiple_of(i * step, step))
+            return 0
+
+        lax.fori_loop(0, total // step, tile, 0)
+
     chunks, tags = [], {}
 
-    def by_rows(buf, source, first, wide):
+    def by_rows(buf, first, wide, parts):
         per = krows // copies
 
         def view(owner, share):
             return buf.at[pl.ds(pl.multiple_of(owner * krows + share * per, per), per), pl.ds(first, wide)]
 
-        return (
-            view,
-            source.at[:, pl.ds(first, wide)],
-            lambda: buf.at[pl.ds(pl.multiple_of(f * krows, krows), krows), pl.ds(first, wide)],
-            per * wide,
-        )
-
-    def by_columns(buf, source, first, wide):
-        deep = buf.shape[0]
+        def fill():
+            loaded(*(k for k, _, _, _ in parts))
+
+            def tile(at):
+                here = pl.ds(pl.multiple_of(f * krows + at, TILE), TILE)
+                for k, source, start, many in parts:
+                    got = staged[k][pl.ds(at, TILE), source : source + many].astype(jnp.bfloat16)
+                    buf[here, start : start + many] = got
+
+            by_tiles(krows, TILE, tile)
+
+        return view, fill, per * wide
+
+    def by_columns(buf, k, scale, first, wide):
+        deep, height = buf.shape[0], staged[k].shape[0]
         per = deep // copies
 
         def view(owner, share):
@@ -88,12 +121,19 @@
                 pl.ds(pl.multiple_of(owner * col + first, LANES), wide),
             ]
 
-        return (
-            view,
-            source.at[:, pl.ds(first, wide)],
-            lambda: buf.at[:, pl.ds(pl.multiple_of(f * col + first, LANES), wide)],
-            per * wide,
-        )
+        def fill():
+            loaded(k)
+            lanes = pl.ds(pl.multiple_of(f * col + first, LANES), wide)
+
+            def tile(at):
+                got = staged[k][pl.ds(at, TILE), first : first + wide] * scale[:, first : first + wide]
+                buf[pl.ds(at, TILE), lanes] = got.astype(jnp.bfloat16)
+
+            by_tiles(height, TILE, tile)
+            if deep > height:
+                buf[height:deep, lanes] = jnp.zeros((deep - height, wide), jnp.bfloat16)
+
+        return view, fill, per * wide
 
     def by_blocks():
         per = 2 * width // copies
@@ -104,84 +144,106 @@
                 pl.ds(pl.multiple_of(share * per, per), per),
             ]
 
-        return (
-            view,
-            wblk,
-            lambda: Wb.at[:, pl.ds(pl.multiple_of(f * brows, brows), brows), :],
-            blocks * brows * per,
-        )
+        def fill():
+            loaded(1, 2)
+            here = pl.ds(pl.multiple_of(f * brows, brows), brows)
+            Wb[:, here, :width] = Fr[...].astype(jnp.bfloat16)
+            Wb[:, here, width:] = Fj[...].astype(jnp.bfloat16)
+
+        return view, fill, blocks * brows * per
+
+    def by_pairs(first, pairs):
+        parts = []
+        for i in range(first, first + pairs):
+            many = min(LANES, ff - i * LANES)
+            parts.append((5, i * LANES, 2 * i * LANES, many))
+            parts.append((6, i * LANES, (2 * i + 1) * LANES, many))
+        return by_rows(Wf, first * 2 * LANES, pairs * 2 * LANES, parts)
+
+    if hid > ff:
+        own_rows = pl.ds(pl.multiple_of(f * krows, krows), krows)
+        Wf[own_rows, 2 * (hid - LANES) : 2 * hid] = jnp.zeros((krows, 2 * LANES), jnp.bfloat16)
 
     def add(tag, chunk):
         tags[tag] = len(chunks)
         chunks.append(chunk)
 
-    add("in", by_rows(Wp, wpair, rec, rec))
     add("blk", by_blocks())
-    add("gate", by_rows(Wp, wpair, 0, rec))
-    add("out", by_columns(Wo, wout, 0, col))
+    add("in", by_rows(Wp, rec, rec, [(0, 0, rec, rec)]))
+    add("gate", by_rows(Wp, 0, rec, [(3, 0, 0, rec)]))
+    add("out", by_columns(Wo, 4, out_scale, 0, col))
     ff_groups, first = [], 0
     for pairs in shares(hid // LANES, 4):
-        add(("ff", len(ff_groups)), by_rows(Wf, wff, first * 2 * LANES, pairs * 2 * LANES))
+        add(("ff", len(ff_groups)), by_pairs(first, pairs))
         ff_groups.append((first, pairs))
         first += pairs
     dn_groups, first = [], 0
     for lanes in shares(col // LANES, 3):
-        add(("dn", len(dn_groups)), by_columns(Wd, wdn, first * LANES, lanes * LANES))
+        add(("dn", len(dn_groups)), by_columns(Wd, 7, down_scale, first * LANES, lanes * LANES))
         dn_groups.append((first * LANES, lanes * LANES))
         first += lanes
 
-    own = []
-    for c, (view, source, place, cost) in enumerate(chunks):
-        own.append(pltpu.make_async_copy(source, place(), own_sem.at[c]))
-        own[c].start()
-    tok = pltpu.make_async_copy(tokens, X.at[t], tok_sem.at[0])
-    tok.start()
-    S[f] = scales[...]
-
+    chunks[0][1]()
     pl.semaphore_wait(barrier, (n - 1) + (copies - 1) + (tp - 1))
 
     drains = []
 
-    def send(copy):
-        copy.start()
-        drains.append(copy)
-
-    def z_copy(c, s):
-        owner = lax.rem(f - s + n, n)
+    def send(copy, when=None):
+        if when is None:
+            copy.start()
+        else:
+            @pl.when(when)
+            def _():
+                copy.start()
+
+        drains.append((copy, when))
+
+    def z_copy(c, owner, side):
         view = chunks[c][0](owner, g)
-        return remote(view, view, z_send.at[c, s], z_recv.at[c, s], "fs", lax.rem(f + 1, n))
-
-    def z_land(c, s):
-        owner = lax.rem(f - s - 1 + n, n)
-        view = chunks[c][0](owner, g)
-        return remote(view, view, z_send.at[c, s], z_recv.at[c, s], "fs", lax.rem(f + 1, n))
-
-    def y_copy(c, s, other, share):
-        owner = lax.rem(f - s + n, n)
+        return remote(
+            view, view, z_send.at[side, c, owner], z_recv.at[c, owner], "fs",
+            jnp.clip(f - 1 if side else f + 1, 0, n - 1),
+        )
+
+    def y_copy(c, owner, other, share):
         view = chunks[c][0](owner, share)
         return remote(
-            view, view, y_send.at[c, s - 1, other - 1], y_recv.at[c, s - 1, other - 1],
+            view, view, y_send.at[c, owner, other - 1], y_recv.at[c, owner, other - 1],
             "grp", lax.rem(g + other, copies),
         )
 
-    def ring_step(c, s):
-        if s == 0:
-            own[c].wait()
-        else:
-            z_land(c, s - 1).wait_recv()
-        if s < n - 1:
-            send(z_copy(c, s))
-        if s > 0:
-            for other in range(1, copies):
-                send(y_copy(c, s, other, g))
-
-    def settled(c, s):
+    def line_step(c, s):
+        if s == 0 and c:
+            chunks[c][1]()
+        for side in range(2):
+            owner = jnp.clip(f + s if side else f - s, 0, n - 1)
+            here = f + s < n if side else f >= s
+            onward = f > 0 if side else f < n - 1
+            if s:
+                @pl.when(here)
+                def _():
+                    z_copy(c, owner, side).wait_recv()
+                    for other in range(1, copies):
+                        y_copy(c, owner, other, g).start()
+
+                for other in range(1, copies):
+                    drains.append((y_copy(c, owner, other, g), here))
+            send(z_copy(c, owner, side), jnp.logical_and(here, onward))
+
+    def settled(c, owner):
         for other in range(1, copies):
-            y_copy(c, s, other, lax.rem(g - other + copies, copies)).wait_recv()
+            y_copy(c, owner, other, lax.rem(g - other + copies, copies)).wait_recv()
 
     def gathered(c):
-        for s in range(1, n):
-            settled(c, s)
+        for k in range(1, n):
+            settled(c, lax.rem(f + k, n))
+
+    def nearest(m):
+        near = jnp.minimum(f, n - 1 - f)
+        two = (m + 1) // 2
+        paired = f - two if m % 2 else f + two
+        single = jnp.where(f < n - 1 - f, f + (m - near), f - (m - near))
+        return jnp.where(m <= 2 * near, paired, single)
 
     def spread(source, buf, sends, recvs):
         for k in range(1, tp):
@@ -193,8 +255,34 @@
             remote(place, place, sends.at[k - 1], recvs.at[k - 1], "tp", lax.rem(t + k, tp)).wait_recv()
 
     spread(tokens, X, x_send, x_recv)
-    for k in range(1, n):
-        send(remote(scales, S.at[f], s_send.at[k - 1], s_recv.at[k - 1], "fs", lax.rem(f + k, n)))
+
+    def send_scales():
+        def placed(scale, wide):
+            many = scale.shape[1]
+            Z[:, :wide] = jnp.zeros((8, wide), jnp.float32)
+            Z[:, :many] = jnp.broadcast_to(scale, (8, many))
+            return pltpu.roll(Z[:, :wide], f * many, 1)[0:1]
+
+        S[f, :, 0:rec] = placed(gate_scale[...], rec)
+        S[f, :, rec : 2 * rec] = placed(in_scale[...], rec)
+        for base, scale in ((2 * rec, recur_scale), (3 * rec, inject_scale)):
+            for block in range(blocks):
+                at = base + block * width
+                S[f, :, at : at + width] = placed(scale[block : block + 1, :], width)
+        for half, scale in enumerate((swish_scale, up_scale)):
+            whole = placed(scale[...], hid)
+            for i in range(hid // LANES):
+                at = 4 * rec + (2 * i + half) * LANES
+                S[f, :, at : at + LANES] = whole[:, i * LANES : (i + 1) * LANES]
+        for k in range(1, n):
+            send(remote(S.at[f], S.at[f], s_send.at[k - 1], s_recv.at[k - 1], "fs", lax.rem(f + k, n)))
+        lost = -decay_param[...]
+        u = jnp.exp(-jnp.abs(lost))
+        z = u / (2.0 + u)
+        square, tail = z * z, 0.0
+        for odd in range(17, 0, -2):
+            tail = tail * square + 1.0 / odd
+        SP[...] = jnp.maximum(lost, 0.0) + 2.0 * z * tail
 
     def norm(buf, gain):
         def tile(i, _):
@@ -240,10 +328,13 @@
     def recurrence():
         gathered(tags["blk"])
         position = lax.broadcasted_iota(jnp.int32, (SEQ_LEN, width), 0)
+        square = (SEQ_LEN, SEQ_LEN)
+        diagonal = lax.broadcasted_iota(jnp.int32, square, 0) == lax.broadcasted_iota(jnp.int32, square, 1)
 
         def sequence(i, _):
             here = pl.ds(pl.multiple_of(i * SEQ_LEN, SEQ_LEN), SEQ_LEN)
-            moved_by = shift[here, :]
+            along = jnp.broadcast_to(shift[pl.ds(i, 1), :], (SEQ_LEN, SEQ_LEN))
+            moved_by = jnp.sum(jnp.where(diagonal, along, 0.0), axis=1, keepdims=True)
             for block in range(blocks):
                 lanes = slice(block * width, (block + 1) * width)
                 at = lambda base: slice(base + block * width, base + (block + 1) * width)
@@ -256,7 +347,7 @@
                 sums = jnp.dot(conv, Wb[block], preferred_element_type=jnp.float32)
                 recur = jax.nn.sigmoid(sums[:, :width] * SV[:, at(2 * rec)])
                 inject = jax.nn.sigmoid(sums[:, width:] * SV[:, at(3 * rec)])
-                log_keep = -8.0 * recur * decay[:, lanes] + moved_by
+                log_keep = -8.0 * recur * SP[:, lanes] + moved_by
                 twice = 2.0 * log_keep
                 near = -twice * (
                     1.0
@@ -278,14 +369,19 @@
 
         lax.fori_loop(0, rows // SEQ_LEN, sequence, 0)
 
+    mixed = []
+
     def mix_out():
         gathered(tags["out"])
         for k in list(range(1, tp)) + [0]:
             peer = lax.rem(t + k, tp)
             lanes = pl.ds(pl.multiple_of(peer * dc, dc), dc)
-            T1[k] = jnp.dot(M[...], Wo[:, lanes], preferred_element_type=jnp.float32).astype(jnp.bfloat16)
+            T[:, lanes] = jnp.dot(M[...], Wo[:, lanes], preferred_element_type=jnp.float32).astype(jnp.bfloat16)
             if k:
-                send(remote(T1.at[k], R1.at[k - 1], r1_send.at[k - 1], r1_recv.at[k - 1], "tp", peer))
+                mixed.append(
+                    remote(T.at[:, lanes], R1.at[k - 1], r1_send.at[k - 1], r1_recv.at[k - 1], "tp", peer)
+                )
+                mixed[-1].start()
 
     def hidden():
         for k in range(1, tp):
@@ -294,7 +390,7 @@
 
         def tile(i, _):
             here = pl.ds(pl.multiple_of(i * SEQ_LEN, SEQ_LEN), SEQ_LEN)
-            total = T1[0, here, :].astype(jnp.float32)
+            total = T[here, pl.ds(pl.multiple_of(t * dc, dc), dc)].astype(jnp.float32)
             for k in range(1, tp):
                 total = total + R1[k - 1, here, :].astype(jnp.float32)
             H[t, here, :] = (X[t, here, :].astype(jnp.float32) + total).astype(jnp.bfloat16)
@@ -307,11 +403,10 @@
         spread_land(H, h_send, h_recv)
         norm(H, gain2)
 
-    def activate(index):
-        first, pairs = ff_groups[index]
-
+    def activate(index, first, pairs, opens):
         def run():
-            gathered(tags[("ff", index)])
+            if opens:
+                gathered(tags[("ff", index)])
 
             def tile(i, _):
                 both = pl.ds(pl.multiple_of((first + i) * 2 * LANES, 2 * LANES), 2 * LANES)
@@ -332,17 +427,20 @@
         first, wide = dn_groups[index]
 
         def run():
+            while mixed:
+                mixed.pop().wait_send()
+            owner = nearest(s)
             if s:
-                settled(tags[("dn", index)], s)
-            start = lax.rem(f - s + n, n) * col + first
+                settled(tags[("dn", index)], owner)
+            start = owner * col + first
             lanes = pl.ds(pl.multiple_of(start, LANES), wide)
             peer = start // dc
             inner = start - peer * dc
-            T2[:, lanes] = jnp.dot(A[...], Wd[:, lanes], preferred_element_type=jnp.float32).astype(jnp.bfloat16)
+            T[:, lanes] = jnp.dot(A[...], Wd[:, lanes], preferred_element_type=jnp.float32).astype(jnp.bfloat16)
 
             def piece():
                 return remote(
-                    T2.at[:, lanes], R2.at[t, :, pl.ds(pl.multiple_of(inner, LANES), wide)],
+                    T.at[:, lanes], R2.at[t, :, pl.ds(pl.multiple_of(inner, LANES), wide)],
                     r2_send.at[index, s], r2_recv.at[t, inner // LANES], "tp", peer,
                 )
 
@@ -365,7 +463,7 @@
 
         def tile(i, _):
             here = pl.ds(pl.multiple_of(i * SEQ_LEN, SEQ_LEN), SEQ_LEN)
-            total = T2[here, pl.ds(pl.multiple_of(t * dc, dc), dc)].astype(jnp.float32)
+            total = T[here, pl.ds(pl.multiple_of(t * dc, dc), dc)].astype(jnp.float32)
             for k in range(1, tp):
                 total = total + R2[lax.rem(t + k, tp), here, :].astype(jnp.float32)
             out[here, :] = (H[t, here, :].astype(jnp.float32) + total).astype(jnp.bfloat16)
@@ -374,13 +472,12 @@
         lax.fori_loop(0, rows // SEQ_LEN, tile, 0)
 
     link = 2 * 2 / 91e3
-    costs = [chunk[3] * link for chunk in chunks]
-    ring, landed = ring_plan(costs, n, 6.0)
+    costs = [chunk[2] * link for chunk in chunks]
+    ring, passed = ring_plan(costs, n, 5.0)
     events = [(when, 0, c, s, None) for when, c, s in ring]
 
     def ready(tag, s=None):
-        c = tags[tag]
-        return landed[(c, (n if s is None else s + 1) - 2)] + costs[c] + 3.0
+        return passed[(tags[tag], n - 1 if s is None else s)]
 
     clock = [0.0]
 
@@ -389,28 +486,37 @@
         events.append((clock[0], 1, len(events), 0, run))
         clock[0] += takes
 
-    across = tp * rows * dc * link / 1.0
-    task(1.0, 0.5, scale_sum)
+    across = tp * rows * dc * link / 2
+    task(3.0, 1.0, send_scales)
+    task(20.0, 0.5, scale_sum)
     task(across, 3.0, first_norm)
-    task(ready("in"), 3.5, project("in", rec))
-    task(ready("gate"), 3.5, project("gate", 0))
-    task(ready("blk"), 7.0, recurrence)
+    task(ready("in"), 2.0, project("in", rec))
+    task(ready("gate"), 2.0, project("gate", 0))
+    task(ready("blk"), 6.0, recurrence)
     task(ready("out"), 4.0, mix_out)
     task(clock[0] + across, 2.0, hidden)
     task(clock[0] + across, 3.0, second_norm)
-    for index in range(len(ff_groups)):
-        task(ready(("ff", index)), 7.0, activate(index))
-    for index in range(len(dn_groups)):
-        for s in range(n):
-            task(ready(("dn", index), s) if s else 0.0, 1.5, down(index, s))
+    for index, (first, pairs) in enumerate(ff_groups):
+        for start in range(0, pairs, 2):
+            many = min(2, pairs - start)
+            task(ready(("ff", index)), 1.0 * many, activate(index, first + start, many, start == 0))
+    last = [(ready(("dn", index), s) if s else 0.0, index, s) for index in range(len(dn_groups)) for s in range(n)]
+    for when, index, s in sorted(last):
+        task(when, 1.3, down(index, s))
     for _, kind, c, s, run in sorted(events, key=lambda e: e[:4]):
         if kind == 0:
-            ring_step(c, s)
+            line_step(c, s)
         else:
             run()
     finish()
-    for copy in drains:
-        copy.wait_send()
+    for copy, when in drains:
+        if when is None:
+            copy.wait_send()
+        else:
+            @pl.when(when)
+            def _(copy=copy):
+                copy.wait_send()
+
     for peer, piece in pieces:
         @pl.when(peer != t)
         def _(piece=piece):
@@ -442,8 +548,6 @@
     down_column_scale,
 ):
     n, copies, tp = (lax.axis_size(axis) for axis in ("fs", "grp", "tp"))
-    f = lax.axis_index("fs")
-    narrow = lambda weight: weight.astype(jnp.bfloat16)
     rows, dc = tokens.shape
     model = dc * tp
     krows, rec = gate_projection_weight.shape
@@ -452,33 +556,18 @@
     hid = -(-ff // LANES) * LANES
     col = output_projection_weight.shape[1]
 
-    def wide(scale):
-        kept = scale.reshape(-1, 1, scale.shape[-1])
-        owner = lax.broadcasted_iota(jnp.int32, (1, n, 1), 1)
-        return jnp.where(owner == f, kept, 0.0).reshape(1, -1)
-
-    def pairs(a, b):
-        pad = ((0, 0), (0, hid - ff))
-        a, b = (jnp.pad(v, pad).reshape(v.shape[0], -1, 1, LANES) for v in (a, b))
-        return jnp.concatenate([a, b], axis=2).reshape(a.shape[0], -1)
-
-    scales = jnp.concatenate(
-        [
-            wide(gate_column_scale),
-            wide(input_column_scale),
-            wide(recurrence_column_scale),
-            wide(input_gate_column_scale),
-            pairs(wide(mixer_gate_column_scale), wide(up_column_scale)),
-        ],
-        axis=1,
+    weights = (
+        input_projection_weight,
+        recurrence_gate_weight,
+        input_gate_weight,
+        gate_projection_weight,
+        output_projection_weight,
+        mixer_gate_weight,
+        up_projection_weight,
+        down_projection_weight,
     )
-    wpair = jnp.concatenate([narrow(gate_projection_weight), narrow(input_projection_weight)], axis=1)
-    wblk = jnp.concatenate([narrow(recurrence_gate_weight), narrow(input_gate_weight)], axis=2)
-    wout = narrow(output_projection_weight * output_column_scale)
-    wff = pairs(narrow(mixer_gate_weight), narrow(up_projection_weight))
-    wdn = jnp.pad(narrow(down_projection_weight * down_column_scale), ((0, hid - ff), (0, 0)))
-
-    dims = (n, copies, tp, rows, model, dc, rec, blocks, brows, width, hid, col)
+
+    dims = (n, copies, tp, rows, model, dc, rec, blocks, brows, width, ff, hid, col)
     chunk_count = 4 + len(shares(hid // LANES, 4)) + len(shares(col // LANES, 3))
     here = pl.BlockSpec(memory_space=pltpu.VMEM)
     away = pl.BlockSpec(memory_space=pl.ANY)
@@ -488,9 +577,17 @@
     return pl.pallas_call(
         lambda *refs: layer_body(dims, *refs),
         out_shape=jax.ShapeDtypeStruct((rows, dc), jnp.bfloat16),
-        in_specs=[away] * 6 + [here] * 6,
+        in_specs=[away] * 9 + [here] * 13,
         out_specs=here,
         scratch_shapes=[
+            pltpu.VMEM(gate_projection_weight.shape, jnp.float32),
+            pltpu.VMEM(input_projection_weight.shape, jnp.float32),
+            pltpu.VMEM(recurrence_gate_weight.shape, jnp.float32),
+            pltpu.VMEM(input_gate_weight.shape, jnp.float32),
+            pltpu.VMEM(output_projection_weight.shape, jnp.float32),
+            pltpu.VMEM(mixer_gate_weight.shape, jnp.float32),
+            pltpu.VMEM(up_projection_weight.shape, jnp.float32),
+            pltpu.VMEM(down_projection_weight.shape, jnp.float32),
             bf(model, 2 * rec),
             bf(blocks, n * brows, 2 * width),
             bf(rec, model),
@@ -501,18 +598,19 @@
             bf(rows, model),
             bf(rows, 2 * rec),
             bf(rows, rec),
-            bf(tp, rows, dc),
+            bf(rows, model),
             bf(tp - 1, rows, dc),
-            bf(rows, model),
             bf(tp, rows, dc),
             bf(rows, hid),
-            pltpu.VMEM((n,) + scales.shape, jnp.float32),
-            pltpu.VMEM(scales.shape, jnp.float32),
-            dma(chunk_count, n - 1),
-            dma(chunk_count, n - 1),
-            dma(chunk_count, n - 1, copies - 1),
-            dma(chunk_count, n - 1, copies - 1),
-            dma(chunk_count),
+            pltpu.VMEM((n, 1, 4 * rec + 2 * hid), jnp.float32),
+            pltpu.VMEM((1, 4 * rec + 2 * hid), jnp.float32),
+            pltpu.VMEM((1, rec), jnp.float32),
+            pltpu.VMEM((8, max(rec, hid)), jnp.float32),
+            dma(2, chunk_count, n),
+            dma(chunk_count, n),
+            dma(chunk_count, n, copies - 1),
+            dma(chunk_count, n, copies - 1),
+            dma(len(weights)),
             dma(1),
             dma(tp - 1),
             dma(tp - 1),
@@ -531,17 +629,20 @@
         cost_estimate=pl.CostEstimate(flops=flops, bytes_accessed=8 * rows * model, transcendentals=0),
     )(
         tokens,
-        wpair,
-        wblk,
-        wout,
-        wff,
-        wdn,
-        scales,
+        *weights,
+        output_column_scale[None, :],
+        down_column_scale[None, :],
+        gate_column_scale[None, :],
+        input_column_scale[None, :],
+        recurrence_column_scale,
+        input_gate_column_scale,
+        mixer_gate_column_scale[None, :],
+        up_column_scale[None, :],
         recurrent_norm_gain[None, :],
         channel_norm_gain[None, :],
         convolution_kernel,
-        jax.nn.softplus(-channel_decay_param)[None, :],
-        position_decay_shift[:, None],
+        channel_decay_param[None, :],
+        position_decay_shift.reshape(-1, SEQ_LEN),
     )
 
 

time: 293 us -> 235 us (0.80)
  Pallas kernels: 260 us -> 227 us
  local copies, waits for them, and re-layouts: 25.1 us -> 4.56 us
  other arithmetic: 7.84 us -> 0 us
    pallas_call x1, Pallas kernels: 260 us -> 227 us  [on_device(): pl.pallas_call(lambda *refs: layer_body(dims, *refs), out_shape=jax.Shape...]
    reshape x1 -> x0, local copies, waits for them, and re-layouts: 7.56 us -> none  [pairs(): return jnp.concatenate([a, b], axis=2).reshape(a.shape[0], -1)]
    unnamed x30 -> x1, local copies, waits for them, and re-layouts: 7.72 us -> 2.06 us
    concatenate x3 -> x0, local copies, waits for them, and re-layouts: 5.56 us -> none  [the longest x2 5.55 us: pairs(): return jnp.concatenate([a, b], axis=2).reshape(a.shape[0], -1)]
    concatenate x4 -> x0, other arithmetic: 3.83 us -> none  [the longest x2 2.07 us: pairs(): return jnp.concatenate([a, b], axis=2).reshape(a.shape[0], -1)]
where the time goes in v1:
time: 235 us; the launch traced here: 232 us
  Pallas kernels  227 us (97%)
  local copies, waits for them, and re-layouts  4.56 us (2%)
    pallas_call x1, Pallas kernels, on_device(): pl.pallas_call(lambda *refs: layer_body(dims, *refs), out_shape=jax.Shape...  227 us

profile of v1, /device:TPU:5, one launch (start us, length us, event | category | flops | bytes accessed | tf_op | source)
XLA Modules:
  0.0 232.0 jit_solution(15489241363210753692)
XLA Ops:
  0.0 1.2 broadcast_in_dim.31.refs_15_
  1.2 1.3 broadcast_in_dim.32.refs_16_
  2.5 227.4 %shard_map.208 = bf16[768,512]{1,0:T(8,128)(2,1)} custom-call(bf16[768,512]{1,0:T(8,128)(2,1)} %refs_0_.1, f32[512,512]{1,0:T(8,128)} %refs_1_.1, f32[2,64,256]{2,1,0:T(8,128)} %refs_2_.1, f32[2,64,256]{2,1,0:T(8,128)} %refs_3_.1, f32[512,512]{1,0:T(8,128)} %refs_4_.1, f32[512,512]{1,0:T(8,128)} %refs_5_.1, f32[512,1408]{1,0:T(8,128)} %refs_6_.1, ...), custom_call_target="tpu_custom_call" | custom-call | flops 18522046464 | bytes 12582912 | tf_op jit(solution)/shard_map/pallas_call | solution.py:577
  229.9 2.1 copy.24

commit v2 on v1

--- a/solution.py
+++ b/solution.py
@@ -19,7 +19,27 @@
     return [total // parts + (1 if i < total % parts else 0) for i in range(parts)]
 
 
-def ring_plan(costs, count, latency):
+def parted(total, parts):
+    spans, first = [], 0
+    for many in shares(total, parts):
+        spans.append((first, many))
+        first += many
+    return spans
+
+
+def solo_rows(deep):
+    return deep * 3 // 8 // LANES * LANES
+
+
+def first_cuts(width):
+    cuts = []
+    for k in (1, 1, 2):
+        if sum(cuts) + k * LANES < width:
+            cuts.append(k * LANES)
+    return cuts + [width - sum(cuts)]
+
+
+def ring_plan(costs, solo, count, latency):
     ready = {(c, 0): 0.0 for c in range(len(costs))}
     free, plan, landed = 0.0, [], {}
     while ready:
@@ -31,16 +51,19 @@
         begin = free
         del ready[(c, s)]
         free = free + costs[c]
-        landed[(c, s)] = free + latency
+        landed[(c, s)] = free + (2.5 if free < 10.0 else latency)
         plan.append((begin, c, s))
         if s + 1 < count - 1:
-            ready[(c, s + 1)] = free + latency
+            ready[(c, s + 1)] = landed[(c, s)]
     for c in range(len(costs)):
         plan.append((landed[(c, count - 2)], c, count - 1))
     passed, free = {}, 0.0
     for when, c, s in sorted((landed[k], k[0], k[1] + 1) for k in landed):
-        free = max(free, when) + costs[c]
-        passed[(c, s)] = free + latency
+        if solo[c]:
+            passed[(c, s)] = when
+        else:
+            free = max(free, when) + costs[c]
+            passed[(c, s)] = free + latency
     return sorted(plan), passed
 
 
@@ -50,9 +73,10 @@
         out_scale, down_scale, gate_scale, in_scale, recur_scale, inject_scale, swish_scale, up_scale,
         gain1, gain2, taps, decay_param, shift, out,
         Fg, Fi, Fr, Fj, Fo, Fs, Fu, Fd,
-        Wp, Wb, Wo, Wf, Wd, X, H, N, UG, M, T, R1, R2, A, S, SV, SP, Z,
+        Wp, Wb, Wo, Wf, Wd, X, H, N, UG, M, T, R1, R2, A, S, SV, SP, Z, B, V, E,
         z_send, z_recv, y_send, y_recv, own_sem, tok_sem,
         x_send, x_recv, r1_send, r1_recv, h_send, h_recv, r2_send, r2_recv, s_send, s_recv,
+        b_send, b_recv, out_sem,
     ) = refs[0], refs[1:9], refs[9:]
     g, f, t = lax.axis_index("grp"), lax.axis_index("fs"), lax.axis_index("tp")
     krows = model // n
@@ -109,31 +133,31 @@
 
             by_tiles(krows, TILE, tile)
 
-        return view, fill, per * wide
-
-    def by_columns(buf, k, scale, first, wide):
-        deep, height = buf.shape[0], staged[k].shape[0]
-        per = deep // copies
+        return view, fill, per * wide, False
+
+    def by_columns(buf, k, scale, first, wide, top=0, bottom=None, solo=False):
+        deep = (buf.shape[0] if bottom is None else bottom) - top
+        height = min(deep, staged[k].shape[0] - top)
+        per = deep if solo else deep // copies
 
         def view(owner, share):
-            return buf.at[
-                pl.ds(pl.multiple_of(share * per, per), per),
-                pl.ds(pl.multiple_of(owner * col + first, LANES), wide),
-            ]
+            start = top if solo else pl.multiple_of(top + share * per, 16)
+            return buf.at[pl.ds(start, per), pl.ds(pl.multiple_of(owner * col + first, LANES), wide)]
 
         def fill():
             loaded(k)
             lanes = pl.ds(pl.multiple_of(f * col + first, LANES), wide)
 
             def tile(at):
-                got = staged[k][pl.ds(at, TILE), first : first + wide] * scale[:, first : first + wide]
-                buf[pl.ds(at, TILE), lanes] = got.astype(jnp.bfloat16)
+                here = pl.ds(pl.multiple_of(top + at, TILE), TILE)
+                got = staged[k][here, first : first + wide] * scale[:, first : first + wide]
+                buf[here, lanes] = got.astype(jnp.bfloat16)
 
             by_tiles(height, TILE, tile)
             if deep > height:
-                buf[height:deep, lanes] = jnp.zeros((deep - height, wide), jnp.bfloat16)
-
-        return view, fill, per * wide
+                buf[top + height : top + deep, lanes] = jnp.zeros((deep - height, wide), jnp.bfloat16)
+
+        return view, fill, per * wide, solo
 
     def by_blocks():
         per = 2 * width // copies
@@ -150,7 +174,7 @@
             Wb[:, here, :width] = Fr[...].astype(jnp.bfloat16)
             Wb[:, here, width:] = Fj[...].astype(jnp.bfloat16)
 
-        return view, fill, blocks * brows * per
+        return view, fill, blocks * brows * per, False
 
     def by_pairs(first, pairs):
         parts = []
@@ -169,8 +193,15 @@
         chunks.append(chunk)
 
     add("blk", by_blocks())
-    add("in", by_rows(Wp, rec, rec, [(0, 0, rec, rec)]))
-    add("gate", by_rows(Wp, 0, rec, [(3, 0, 0, rec)]))
+    def add_projection(tag, k, base, cuts):
+        start = 0
+        for i, wide in enumerate(cuts):
+            add((tag, i), by_rows(Wp, base + start, wide, [(k, start, base + start, wide)]))
+            start += wide
+
+    in_cuts, gate_cuts = first_cuts(rec), [LANES * k for k in shares(rec // LANES, 2)]
+    add_projection("in", 0, rec, in_cuts)
+    add_projection("gate", 3, 0, gate_cuts)
     add("out", by_columns(Wo, 4, out_scale, 0, col))
     ff_groups, first = [], 0
     for pairs in shares(hid // LANES, 4):
@@ -179,7 +210,11 @@
         first += pairs
     dn_groups, first = [], 0
     for lanes in shares(col // LANES, 3):
-        add(("dn", len(dn_groups)), by_columns(Wd, 7, down_scale, first * LANES, lanes * LANES))
+        index, at, wide = len(dn_groups), first * LANES, lanes * LANES
+        cut = solo_rows(hid) if index == len(shares(col // LANES, 3)) - 1 else 0
+        add(("dn", index), by_columns(Wd, 7, down_scale, at, wide, cut, hid))
+        if cut:
+            add("solo", by_columns(Wd, 7, down_scale, at, wide, 0, cut, True))
         dn_groups.append((first * LANES, lanes * LANES))
         first += lanes
 
@@ -211,6 +246,9 @@
             view, view, y_send.at[c, owner, other - 1], y_recv.at[c, owner, other - 1],
             "grp", lax.rem(g + other, copies),
         )
+
+    def passing(c):
+        return range(1, 1 if chunks[c][3] else copies)
 
     def line_step(c, s):
         if s == 0 and c:
@@ -223,15 +261,15 @@
                 @pl.when(here)
                 def _():
                     z_copy(c, owner, side).wait_recv()
-                    for other in range(1, copies):
+                    for other in passing(c):
                         y_copy(c, owner, other, g).start()
 
-                for other in range(1, copies):
+                for other in passing(c):
                     drains.append((y_copy(c, owner, other, g), here))
             send(z_copy(c, owner, side), jnp.logical_and(here, onward))
 
     def settled(c, owner):
-        for other in range(1, copies):
+        for other in passing(c):
             y_copy(c, owner, other, lax.rem(g - other + copies, copies)).wait_recv()
 
     def gathered(c):
@@ -258,7 +296,8 @@
 
     def send_scales():
         def placed(scale, wide):
-            many = scale.shape[1]
+            many = scale.shape[-1]
+            scale = scale.reshape(1, many)
             Z[:, :wide] = jnp.zeros((8, wide), jnp.float32)
             Z[:, :many] = jnp.broadcast_to(scale, (8, many))
             return pltpu.roll(Z[:, :wide], f * many, 1)[0:1]
@@ -302,9 +341,10 @@
         spread_land(X, x_send, x_recv)
         norm(X, gain1)
 
-    def project(tag, first):
+    def project(tag, cuts, first):
         def run():
-            gathered(tags[tag])
+            for i in range(len(cuts)):
+                gathered(tags[(tag, i)])
 
             def tile(i, _):
                 lanes = pl.ds(pl.multiple_of(first + i * 256, LANES), 256)
@@ -325,8 +365,12 @@
             total = total + S[o]
         SV[...] = total
 
-    def recurrence():
-        gathered(tags["blk"])
+    def recurrence(first, many):
+        return lambda: sequences_of(first, many)
+
+    def sequences_of(first, many):
+        if first == 0:
+            gathered(tags["blk"])
         position = lax.broadcasted_iota(jnp.int32, (SEQ_LEN, width), 0)
         square = (SEQ_LEN, SEQ_LEN)
         diagonal = lax.broadcasted_iota(jnp.int32, square, 0) == lax.broadcasted_iota(jnp.int32, square, 1)
@@ -367,7 +411,7 @@
                 M[here, lanes] = (jax.nn.gelu(gate) * state).astype(jnp.bfloat16)
             return 0
 
-        lax.fori_loop(0, rows // SEQ_LEN, sequence, 0)
+        lax.fori_loop(first, first + many, sequence, 0)
 
     mixed = []
 
@@ -421,7 +465,45 @@
 
         return run
 
-    pieces = []
+    pieces, held = [], []
+    chip, core, chips = t // 2, lax.rem(t, 2), tp // 2
+    half = rows // 2
+    mine = pl.ds(pl.multiple_of(core * half, half), half)
+    theirs = pl.ds(pl.multiple_of((1 - core) * half, half), half)
+    partner = t + 1 - 2 * core
+
+    def launch(when, make):
+        @pl.when(when)
+        def _():
+            make().start()
+
+        pieces.append((when, make))
+
+    def add_up():
+        while held:
+            index, s, lanes, peer, place = held.pop()
+            away = peer // 2 != chip
+
+            def onward():
+                return remote(
+                    V.at[:, lanes], R2.at[chip, mine, place],
+                    r2_send.at[index, s], r2_recv.at[chip, core, place_index(place)], "tp", peer,
+                )
+
+            @pl.when(away)
+            def _():
+                remote(
+                    B.at[:, lanes], B.at[:, lanes], b_send.at[index, s], b_recv.at[index, s], "tp", partner
+                ).wait_recv()
+                V[:, lanes] = (T[mine, lanes].astype(jnp.float32) + B[:, lanes].astype(jnp.float32)).astype(
+                    jnp.bfloat16
+                )
+                onward().start()
+
+            pieces.append((away, onward))
+
+    def place_index(place):
+        return place.start // LANES
 
     def down(index, s):
         first, wide = dn_groups[index]
@@ -429,51 +511,61 @@
         def run():
             while mixed:
                 mixed.pop().wait_send()
+            add_up()
             owner = nearest(s)
             if s:
                 settled(tags[("dn", index)], owner)
             start = owner * col + first
             lanes = pl.ds(pl.multiple_of(start, LANES), wide)
             peer = start // dc
-            inner = start - peer * dc
+            place = pl.ds(pl.multiple_of(start - peer * dc, LANES), wide)
             T[:, lanes] = jnp.dot(A[...], Wd[:, lanes], preferred_element_type=jnp.float32).astype(jnp.bfloat16)
-
-            def piece():
-                return remote(
-                    T.at[:, lanes], R2.at[t, :, pl.ds(pl.multiple_of(inner, LANES), wide)],
-                    r2_send.at[index, s], r2_recv.at[t, inner // LANES], "tp", peer,
-                )
-
-            @pl.when(peer != t)
-            def _():
-                piece().start()
-
-            pieces.append((peer, piece))
+            launch(
+                peer == partner,
+                lambda: remote(
+                    T.at[:, lanes], R2.at[chip, :, place],
+                    r2_send.at[index, s], r2_recv.at[chip, 0, place_index(place)], "tp", partner,
+                ),
+            )
+            launch(
+                peer // 2 != chip,
+                lambda: remote(
+                    T.at[theirs, lanes], B.at[:, lanes], b_send.at[index, s], b_recv.at[index, s], "tp", partner
+                ),
+            )
+            held.append((index, s, lanes, peer, place))
 
         return run
 
     def finish():
-        for k in range(1, tp):
-            peer = lax.rem(t + k, tp)
-            for part in range(dc // col):
-                for first, wide in dn_groups:
-                    inner = part * col + first
-                    place = R2.at[peer, :, pl.ds(inner, wide)]
-                    remote(place, place, r2_send.at[0, 0], r2_recv.at[peer, inner // LANES], "tp", peer).wait_recv()
-
-        def tile(i, _):
-            here = pl.ds(pl.multiple_of(i * SEQ_LEN, SEQ_LEN), SEQ_LEN)
+        add_up()
+        for part in range(dc // col):
+            for first, wide in dn_groups:
+                place = pl.ds(part * col + first, wide)
+                at = place_index(place)
+                whole = R2.at[chip, :, place]
+                remote(whole, whole, r2_send.at[0, 0], r2_recv.at[chip, 0, at], "tp", partner).wait_recv()
+                for k in range(1, chips):
+                    other = lax.rem(chip + k, chips)
+                    for h in range(2):
+                        piece = R2.at[other, h * half : (h + 1) * half, place]
+                        remote(piece, piece, r2_send.at[0, 0], r2_recv.at[other, h, at], "tp", partner).wait_recv()
+
+        writes = []
+        for i in range(rows // SEQ_LEN):
+            here = slice(i * SEQ_LEN, (i + 1) * SEQ_LEN)
             total = T[here, pl.ds(pl.multiple_of(t * dc, dc), dc)].astype(jnp.float32)
-            for k in range(1, tp):
-                total = total + R2[lax.rem(t + k, tp), here, :].astype(jnp.float32)
-            out[here, :] = (H[t, here, :].astype(jnp.float32) + total).astype(jnp.bfloat16)
-            return 0
-
-        lax.fori_loop(0, rows // SEQ_LEN, tile, 0)
+            for k in range(chips):
+                total = total + R2[k, here, :].astype(jnp.float32)
+            E[here, :] = (H[t, here, :].astype(jnp.float32) + total).astype(jnp.bfloat16)
+            writes.append(pltpu.make_async_copy(E.at[here, :], out.at[here, :], out_sem.at[i]))
+            writes[-1].start()
+        for write in writes:
+            write.wait()
 
     link = 2 * 2 / 91e3
     costs = [chunk[2] * link for chunk in chunks]
-    ring, passed = ring_plan(costs, n, 5.0)
+    ring, passed = ring_plan(costs, [chunk[3] for chunk in chunks], n, 5.0)
     events = [(when, 0, c, s, None) for when, c, s in ring]
 
     def ready(tag, s=None):
@@ -490,17 +582,26 @@
     task(3.0, 1.0, send_scales)
     task(20.0, 0.5, scale_sum)
     task(across, 3.0, first_norm)
-    task(ready("in"), 2.0, project("in", rec))
-    task(ready("gate"), 2.0, project("gate", 0))
-    task(ready("blk"), 6.0, recurrence)
-    task(ready("out"), 4.0, mix_out)
+    spare = 3.0
+    task(ready(("in", len(in_cuts) - 1)) + spare, 2.0, project("in", in_cuts, rec))
+    task(ready(("gate", len(gate_cuts) - 1)) + spare, 2.0, project("gate", gate_cuts, 0))
+    sequences = rows // SEQ_LEN
+    for first, many in parted(sequences, 3):
+        task(ready("blk"), 6.0 * many / sequences, recurrence(first, many))
+    task(ready("out") + spare, 3.0, mix_out)
     task(clock[0] + across, 2.0, hidden)
     task(clock[0] + across, 3.0, second_norm)
     for index, (first, pairs) in enumerate(ff_groups):
         for start in range(0, pairs, 2):
             many = min(2, pairs - start)
-            task(ready(("ff", index)), 1.0 * many, activate(index, first + start, many, start == 0))
-    last = [(ready(("dn", index), s) if s else 0.0, index, s) for index in range(len(dn_groups)) for s in range(n)]
+            task(ready(("ff", index)) + spare, 1.0 * many, activate(index, first + start, many, start == 0))
+    def arrived(index, s):
+        if s == 0:
+            return 0.0
+        whole = ready(("dn", index), s)
+        return max(whole, ready("solo", s)) if index == len(dn_groups) - 1 else whole
+
+    last = [(arrived(index, s), index, s) for index in range(len(dn_groups)) for s in range(n)]
     for when, index, s in sorted(last):
         task(when, 1.3, down(index, s))
     for _, kind, c, s, run in sorted(events, key=lambda e: e[:4]):
@@ -517,10 +618,10 @@
             def _(copy=copy):
                 copy.wait_send()
 
-    for peer, piece in pieces:
-        @pl.when(peer != t)
-        def _(piece=piece):
-            piece().wait_send()
+    for when, make in pieces:
+        @pl.when(when)
+        def _(make=make):
+            make().wait_send()
 
 
 def on_device(
@@ -568,7 +669,7 @@
     )
 
     dims = (n, copies, tp, rows, model, dc, rec, blocks, brows, width, ff, hid, col)
-    chunk_count = 4 + len(shares(hid // LANES, 4)) + len(shares(col // LANES, 3))
+    chunk_count = 3 + len(first_cuts(rec)) + len(shares(rec // LANES, 2)) + len(shares(hid // LANES, 4)) + len(shares(col // LANES, 3))
     here = pl.BlockSpec(memory_space=pltpu.VMEM)
     away = pl.BlockSpec(memory_space=pl.ANY)
     bf = lambda *shape: pltpu.VMEM(shape, jnp.bfloat16)
@@ -578,7 +679,7 @@
         lambda *refs: layer_body(dims, *refs),
         out_shape=jax.ShapeDtypeStruct((rows, dc), jnp.bfloat16),
         in_specs=[away] * 9 + [here] * 13,
-        out_specs=here,
+        out_specs=away,
         scratch_shapes=[
             pltpu.VMEM(gate_projection_weight.shape, jnp.float32),
             pltpu.VMEM(input_projection_weight.shape, jnp.float32),
@@ -600,12 +701,15 @@
             bf(rows, rec),
             bf(rows, model),
             bf(tp - 1, rows, dc),
-            bf(tp, rows, dc),
+            bf(tp // 2, rows, dc),
             bf(rows, hid),
             pltpu.VMEM((n, 1, 4 * rec + 2 * hid), jnp.float32),
             pltpu.VMEM((1, 4 * rec + 2 * hid), jnp.float32),
             pltpu.VMEM((1, rec), jnp.float32),
             pltpu.VMEM((8, max(rec, hid)), jnp.float32),
+            bf(rows // 2, model),
+            bf(rows // 2, model),
+            bf(rows, dc),
             dma(2, chunk_count, n),
             dma(chunk_count, n),
             dma(chunk_count, n, copies - 1),
@@ -619,9 +723,12 @@
             dma(tp - 1),
             dma(tp - 1),
             dma(len(shares(col // LANES, 3)), n),
-            dma(tp, dc // LANES),
+            dma(tp // 2, 2, dc // LANES),
             dma(n - 1),
             dma(n - 1),
+            dma(len(shares(col // LANES, 3)), n),
+            dma(len(shares(col // LANES, 3)), n),
+            dma(rows // SEQ_LEN),
         ],
         compiler_params=pltpu.CompilerParams(
             collective_id=0, has_side_effects=True, vmem_limit_bytes=67_043_328
@@ -636,8 +743,8 @@
         input_column_scale[None, :],
         recurrence_column_scale,
         input_gate_column_scale,
-        mixer_gate_column_scale[None, :],
-        up_column_scale[None, :],
+        mixer_gate_column_scale,
+        up_column_scale,
         recurrent_norm_gain[None, :],
         channel_norm_gain[None, :],
         convolution_kernel,

time: 235 us -> 222 us (0.945)
  Pallas kernels: 227 us -> 217 us
  local copies, waits for them, and re-layouts: 4.56 us -> 2.06 us
    pallas_call x1, Pallas kernels: 227 us -> 217 us  [on_device(): pl.pallas_call(lambda *refs: layer_body(dims, *refs), out_shape=jax.Shape...]
    broadcast_in_dim x2 -> x0, local copies, waits for them, and re-layouts: 2.5 us -> none  [the longest x1 1.26 us: on_device(): up_column_scale[None, :]]
where the time goes in v2:
time: 222 us; the launch traced here: 219 us
  Pallas kernels  217 us (98%)
    pallas_call x1, Pallas kernels, on_device(): pl.pallas_call(lambda *refs: layer_body(dims, *refs), out_shape=jax.Shape...  217 us

profile of v2, /device:TPU:5, one launch (start us, length us, event | category | flops | bytes accessed | tf_op | source)
XLA Modules:
  0.0 219.1 jit_solution(1556261193056317988)
XLA Ops:
  0.0 217.1 %shard_map.208 = bf16[768,512]{1,0:T(8,128)(2,1)} custom-call(bf16[768,512]{1,0:T(8,128)(2,1)} %refs_0_.1, f32[512,512]{1,0:T(8,128)} %refs_1_.1, f32[2,64,256]{2,1,0:T(8,128)} %refs_2_.1, f32[2,64,256]{2,1,0:T(8,128)} %refs_3_.1, f32[512,512]{1,0:T(8,128)} %refs_4_.1, f32[512,512]{1,0:T(8,128)} %refs_5_.1, f32[512,1408]{1,0:T(8,128)} %refs_6_.1, ...), custom_call_target="tpu_custom_call" | custom-call | flops 18522046464 | bytes 12582912 | tf_op jit(solution)/shard_map/pallas_call | solution.py:678
  217.1 2.1 copy.24

commit v3 on v2

--- a/solution.py
+++ b/solution.py
@@ -563,9 +563,9 @@
         for write in writes:
             write.wait()
 
-    link = 2 * 2 / 91e3
+    link = 2 * 2 / 93.5e3
     costs = [chunk[2] * link for chunk in chunks]
-    ring, passed = ring_plan(costs, [chunk[3] for chunk in chunks], n, 5.0)
+    ring, passed = ring_plan(costs, [chunk[3] for chunk in chunks], n, 4.0)
     events = [(when, 0, c, s, None) for when, c, s in ring]
 
     def ready(tag, s=None):

time: 222 us -> 222 us (level)
  no operation moved by 1% of the time
where the time goes in v3:
time: 222 us; the launch traced here: 219 us
  Pallas kernels  217 us (98%)
    pallas_call x1, Pallas kernels, on_device(): pl.pallas_call(lambda *refs: layer_body(dims, *refs), out_shape=jax.Shape...  217 us

profile of v3, /device:TPU:5, one launch (start us, length us, event | category | flops | bytes accessed | tf_op | source)
XLA Modules:
  0.0 219.1 jit_solution(13891644294886768158)
XLA Ops:
  0.0 217.1 %shard_map.208 = bf16[768,512]{1,0:T(8,128)(2,1)} custom-call(bf16[768,512]{1,0:T(8,128)(2,1)} %refs_0_.1, f32[512,512]{1,0:T(8,128)} %refs_1_.1, f32[2,64,256]{2,1,0:T(8,128)} %refs_2_.1, f32[2,64,256]{2,1,0:T(8,128)} %refs_3_.1, f32[512,512]{1,0:T(8,128)} %refs_4_.1, f32[512,512]{1,0:T(8,128)} %refs_5_.1, f32[512,1408]{1,0:T(8,128)} %refs_6_.1, ...), custom_call_target="tpu_custom_call" | custom-call | flops 18522046464 | bytes 12582912 | tf_op jit(solution)/shard_map/pallas_call | solution.py:678
  217.1 2.1 copy.24
